TPU v7x, 32 devices: a whole 2x2x4 slice. The times are simulated.
32 devices in a mesh: grp: 2 (over y), sp: 4 (over z), tp: 4 (over x, core).
Axes of the slice: x: 2, y: 2, z: 4, core: 2. Of those that a mesh axis runs over, the one named last changes fastest.
Arguments:
- prompt_rows: bfloat16 [6144, 2048], P(('grp', 'sp')), parts along dimension 0, may hold values from -6 to 6
- norm_gain: float32 [2048], replicated, may hold values from 0.1 to 1.9
- key_weight: bfloat16 [2048, 1024], P(None, 'tp'), may hold values from -0.125 to 0.125
- value_weight: bfloat16 [2048, 1024], P(None, 'tp'), may hold values from -0.125 to 0.125
- new_query: bfloat16 [2048], P(('grp', 'tp')), parts along dimension 0, may hold values from -6 to 6
- score_offset: float32 [16], P('tp'), may hold values from -11.5 to -4
- output_gain: float32 [1024], P('tp'), may hold values from 0.1 to 1.9
Outputs:
- key_cache: bfloat16 [8, 4, 4, 768, 64], P(('grp', 'tp'), 'sp'), parts along dimension 0
- value_cache: bfloat16 [8, 4, 4, 768, 64], P(('grp', 'tp'), 'sp'), parts along dimension 0
- first_read: bfloat16 [2048], P(('grp', 'tp')), parts along dimension 0
There are 2 independent parts, one for each index of `grp`. A program takes and returns all parts, laid end to end along the dimension named above; an argument that names none is the same for every part. Nothing has to cross between parts.
All inputs are finite; a program needn't handle non-finite values.
Results may differ from a plain program's by a relative error of at most 0.0059.
Values may be sent and summed in bfloat16 or wider, within the bound.
A program may use at most 64 MiB of HBM per device.

v0:
```python
import jax
import jax.numpy as jnp
from jax import lax
from jax.sharding import PartitionSpec as P

EPSILON = 1e-06


def prefix(value, axis, combine, identity):
    peers, position = (lax.axis_size(axis), lax.axis_index(axis))
    everything = lax.all_gather(value, axis)
    start = jnp.broadcast_to(jnp.asarray(identity, value.dtype), value.shape)

    def hop(k, before):
        at = peers - 1 - k
        reached = at > position
        new = combine(before, everything[at])
        return jnp.where(reached, new, before)

    return lax.fori_loop(0, peers, hop, start)


def normalize(rows, norm_gain):
    rows32 = rows.astype(jnp.float32)
    mean_square = jnp.mean(rows32 * rows32, axis=-1, keepdims=True)
    return (rows32 * lax.rsqrt(mean_square + EPSILON) * norm_gain).astype(jnp.bfloat16)


def project_rows(rows, norm_gain, key_weight, value_weight):
    normed = normalize(rows, norm_gain)
    keys = jnp.dot(normed, key_weight, preferred_element_type=jnp.float32).astype(jnp.bfloat16)
    values = jnp.dot(normed, value_weight, preferred_element_type=jnp.float32).astype(jnp.bfloat16)
    return (keys, values)


def cache_layout(keys, values, head_count):
    devices = lax.axis_size("sp")
    subs = devices // head_count
    depth = keys.shape[1] // head_count
    rows = keys.shape[0] // subs

    def arrange(cache):
        split = cache.reshape(subs, rows, head_count, depth)
        return jnp.transpose(split, (2, 0, 1, 3)).reshape(devices, 1, rows, depth)

    moved_keys, moved_values = (
        lax.all_to_all(arrange(keys), "sp", split_axis=0, concat_axis=1, tiled=True),
        lax.all_to_all(arrange(values), "sp", split_axis=0, concat_axis=1, tiled=True),
    )
    target = (1, 1, devices, rows, depth)
    return (moved_keys.reshape(target), moved_values.reshape(target))


def add_terms(first_part, second_part):
    return first_part + second_part


def read_early(new_query, keys, values, score_offset):
    head_count = score_offset.shape[0]
    depth = keys.shape[1] // head_count
    query2 = new_query.reshape(head_count, depth)
    keys3 = keys.reshape(keys.shape[0], head_count, depth)
    scores = jnp.einsum("hd,shd->hs", query2, keys3, preferred_element_type=jnp.float32)
    scores = scores * depth ** (-0.5) + score_offset[:, None]
    remain = jax.nn.log_sigmoid(-scores)
    within = lax.cumsum(remain, axis=1, reverse=True) - remain
    totals = jnp.sum(remain, axis=1)
    beyond = prefix(totals, "sp", add_terms, jnp.zeros_like(totals))
    sticks = jnp.exp(jax.nn.log_sigmoid(scores) + within + beyond[:, None]).astype(jnp.bfloat16)
    values3 = values.reshape(values.shape[0], head_count, depth)
    partial_value = jnp.einsum("hs,shd->hd", sticks, values3, preferred_element_type=jnp.float32)
    return lax.psum(partial_value, "sp")


def finish_read(mixed, output_gain, head_count):
    spread = jnp.mean(mixed * mixed, axis=-1, keepdims=True)
    result = mixed * lax.rsqrt(spread + EPSILON) * output_gain.reshape(head_count, -1)
    return result.reshape(-1).astype(jnp.bfloat16)


def body(prompt_rows, norm_gain, key_weight, value_weight, new_query, score_offset, output_gain):
    head_count = score_offset.shape[0]
    keys_here, values_here = project_rows(prompt_rows, norm_gain, key_weight, value_weight)
    keys_all, values_all = cache_layout(keys_here, values_here, head_count)
    local_keys, local_values = project_rows(prompt_rows, norm_gain, key_weight, value_weight)
    mixed = read_early(new_query, local_keys, local_values, score_offset)
    return (keys_all, values_all, finish_read(mixed, output_gain, head_count))


def solution(mesh):
    in_specs = (
        P(("grp", "sp"), None),
        P(),
        P(None, "tp"),
        P(None, "tp"),
        P(("grp", "tp")),
        P("tp"),
        P("tp"),
    )
    out_specs = (
        P(("grp", "tp"), "sp", None, None, None),
        P(("grp", "tp"), "sp", None, None, None),
        P(("grp", "tp")),
    )
    return jax.shard_map(body, mesh=mesh, in_specs=in_specs, out_specs=out_specs, check_vma=False)
```

profile of v0, /device:TPU:0, one launch (start us, length us, event | category | flops | bytes accessed | tf_op | source)
XLA Modules:
  0.0 56.2 jit_solution(451119704450405001)
XLA Ops:
  0.6 0.0 copy-start
  0.6 0.0 copy-start.1
  0.7 2.7 %fusion = f32[768]{0:T(1024)S(1)} fusion(bf16[768,2048]{1,0:T(8,128)(2,1)} %param.9), kind=kLoop, calls=%fused_computation.4 | loop fusion | flops 4717824 | bytes 3148800 | tf_op jit(solution)/shard_map/reduce_sum | solution.py:25
  3.4 0.4 copy-done.1
  3.8 0.0 copy-start.5
  3.8 2.1 %convolution_convert_fusion.1 = bf16[768,256]{0,1:T(8,128)(2,1)} fusion(bf16[2048,256]{1,0:T(8,128)(2,1)S(1)} %copy-done, bf16[768,2048]{1,0:T(8,128)(2,1)S(1)} %copy-done.1, f32[2048]{0:T(1024)S(1)} %copy-done.6, f32[768]{0:T(1024)S(1)} %add_rsqrt_fusion), kind=kOutput, calls=%fused_computation.8 | convolution fusion | flops 811794432 | bytes 4598784 | tf_op jit(solution)/shard_map/dot_general | solution.py:31
  5.9 6.3 %all-to-all-start = ((bf16[4,1,768,64]{2,3,1,0:T(8,128)(2,1)}), bf16[4,1,768,64]{2,3,1,0:T(8,128)(2,1)S(1)}, u32[]{:S(2)}, u32[]{:S(2)}) async-start(bf16[4,1,768,64]{2,3,1,0:T(8,128)(2,1)} %bitcast.2), calls=%async_computation | async-start | bytes 786432 | tf_op jit(solution)/shard_map/all_to_all | solution.py:47
  12.3 0.1 reshape.98
  12.4 1.2 %fusion.16 = f32[4,1,768]{2,1,0:T(1,128)S(1)} fusion(bf16[768,4,64]{0,2,1:T(8,128)(2,1)} %bitcast.8, bf16[4,64,1]{1,2,0:T(2,128)(2,1)S(1)} %reshape.98), kind=kOutput, calls=%fused_computation.31 | convolution fusion | flops 393216 | bytes 406016 | tf_op jit(solution)/shard_map/hd,shd->hs/dot_general | solution.py:63
  13.5 0.2 fusion.15
  13.7 5.0 %reduce-window.6 = f32[4,6,128]{2,1,0:T(8,128)S(1)} reduce-window(f32[4,6,128]{2,1,0:T(8,128)S(1)} %reshape.83, f32[]{:T(128)} %constant.61.clone.1), window={size=1x1x128 pad=0_0x0_0x0_127}, to_apply=%region_1.0 | reduce-window | flops 390144 | bytes 24580 | tf_op jit(solution)/shard_map/reduce-window
  18.7 0.1 slice_reduce_fusion
  18.8 0.2 reduce-window.9
  19.0 0.1 slice.7
  19.1 0.1 add_bitcast_fusion
  19.1 0.6 %dynamic-slice = u32[1]{0:T(128)} dynamic-slice(u32[32]{0:T(128)S(1)} %copy-done.7, u32[]{:T(128)S(6)} %add.95), dynamic_slice_sizes={1} | dynamic-slice | bytes 12
  20.4 0.1 negate_dynamic-update-slice_fusion
  20.5 12.2 %all-reduce = f32[16]{0:T(128)S(1)} all-reduce(f32[16]{0:T(128)S(1)} %negate_dynamic-update-slice_fusion), channel_id=2, replica_groups=mesh['grp'=2,'sp'=4,'tp'=4] {'sp'}, use_global_device_ids=true, to_apply=%add | all-reduce | flops 16 | bytes 128
  32.6 0.1 reshape.87
  32.7 0.1 while.16
  32.9 0.1 fusion.13
  33.0 0.0 copy-start.3
  33.0 3.9 %convolution_convert_fusion = bf16[768,256]{0,1:T(8,128)(2,1)} fusion(bf16[2048,256]{1,0:T(8,128)(2,1)S(1)} %copy-done.5, bf16[768,2048]{1,0:T(8,128)(2,1)} %param.9, f32[2048]{0:T(1024)S(1)} %copy-done.6, f32[768]{0:T(1024)S(1)} %add_rsqrt_fusion), kind=kOutput, calls=%fused_computation.7 | convolution fusion | flops 811794432 | bytes 4598784 | tf_op jit(solution)/shard_map/dot_general | solution.py:32
  36.9 3.5 %all-to-all-start.1 = ((bf16[4,1,768,64]{2,3,1,0:T(8,128)(2,1)}), bf16[4,1,768,64]{2,3,1,0:T(8,128)(2,1)S(1)}, u32[]{:S(2)}, u32[]{:S(2)}) async-start(bf16[4,1,768,64]{2,3,1,0:T(8,128)(2,1)} %bitcast.6), calls=%async_computation.1 | async-start | bytes 786432 | tf_op jit(solution)/shard_map/all_to_all | solution.py:48
  40.4 1.2 %fusion.11 = f32[4,1,64]{2,1,0:T(1,128)S(1)} fusion(bf16[768,4,64]{0,2,1:T(8,128)(2,1)} %bitcast.12, bf16[4,768,1]{1,0,2:T(4,128)(2,1)S(1)} %fusion.13), kind=kOutput, calls=%fused_computation.21 | convolution fusion | flops 393216 | bytes 400384 | tf_op jit(solution)/shard_map/hs,shd->hd/dot_general | solution.py:71
  41.6 0.1 reshape.86
  41.7 12.1 %psum.7 = f32[4,64]{1,0:T(4,128)S(1)} all-reduce(f32[4,64]{1,0:T(4,128)S(1)} %bitcast.54), channel_id=1, replica_groups=mesh['grp'=2,'sp'=4,'tp'=4] {'sp'}, use_global_device_ids=true, to_apply=%region_6.7 | all-reduce | flops 256 | bytes 2048 | tf_op jit(solution)/shard_map/psum | solution.py:72
  53.9 0.1 multiply_reduce_fusion
  54.0 0.1 multiply_convert_fusion
  54.1 0.6 %convert_element_type.31 = bf16[256]{0:T(256)(128)(2,1)} reshape(bf16[4,64]{1,0:T(4,128)(2,1)S(1)} %multiply_convert_fusion) | data formatting | bytes 1024 | tf_op jit(solution)/shard_map/convert_element_type | solution.py:78
  54.7 0.7 %copy.46 = bf16[1,1,4,768,64]{3,4,2,1,0:T(8,128)(2,1)} copy(bf16[1,1,4,768,64]{3,4,2,1,0:T(8,128)(2,1)S(1)} %bitcast.52) | data formatting | bytes 786432
  55.4 0.7 %copy.47 = bf16[1,1,4,768,64]{3,4,2,1,0:T(8,128)(2,1)} copy(bf16[1,1,4,768,64]{3,4,2,1,0:T(8,128)(2,1)S(1)} %bitcast.53) | data formatting | bytes 786432
  (22 shorter events, 0.1 us)
Async XLA Ops:
  0.6 2.8 %copy-start = (bf16[2048,256]{1,0:T(8,128)(2,1)S(1)}, bf16[2048,256]{1,0:T(8,128)(2,1)}, u32[]{:S(2)}) copy-start(bf16[2048,256]{1,0:T(8,128)(2,1)} %param.11) | copy-start | bytes 3145732
  0.6 3.2 %copy-start.1 = (bf16[768,2048]{1,0:T(8,128)(2,1)S(1)}, bf16[768,2048]{1,0:T(8,128)(2,1)}, u32[]{:S(2)}) copy-start(bf16[768,2048]{1,0:T(8,128)(2,1)} %param.9) | copy-start | bytes 9437188
  0.7 3.1 %copy-start.6 = (f32[2048]{0:T(1024)S(1)}, f32[2048]{0:T(1024)}, u32[]{:S(2)}) copy-start(f32[2048]{0:T(1024)} %param.10) | copy-start | bytes 24580
  3.8 8.5 %copy-start.4 = (bf16[256]{0:T(256)(128)(2,1)S(1)}, bf16[256]{0:T(256)(128)(2,1)}, u32[]{:S(2)}) copy-start(bf16[256]{0:T(256)(128)(2,1)} %param.13) | copy-start | bytes 1540
  3.8 9.7 %copy-start.2 = (f32[4]{0:T(128)S(1)}, f32[4]{0:T(128)}, u32[]{:S(2)}) copy-start(f32[4]{0:T(128)} %param.14) | copy-start | bytes 52
  3.8 15.3 %copy-start.7 = (u32[32]{0:T(128)S(1)}, u32[32]{0:T(128)}, u32[]{:S(2)}) copy-start(u32[32]{0:T(128)} %constant.71) | copy-start | bytes 388
  3.8 29.2 %copy-start.5 = (bf16[2048,256]{1,0:T(8,128)(2,1)S(1)}, bf16[2048,256]{1,0:T(8,128)(2,1)}, u32[]{:S(2)}) copy-start(bf16[2048,256]{1,0:T(8,128)(2,1)} %param.12) | copy-start | bytes 3145732
  5.9 31.0 %all-to-all-start = ((bf16[4,1,768,64]{2,3,1,0:T(8,128)(2,1)}), bf16[4,1,768,64]{2,3,1,0:T(8,128)(2,1)S(1)}, u32[]{:S(2)}, u32[]{:S(2)}) async-start(bf16[4,1,768,64]{2,3,1,0:T(8,128)(2,1)} %bitcast.2), calls=%async_computation | async-start | bytes 786432 | tf_op jit(solution)/shard_map/all_to_all | solution.py:47
  33.0 8.6 %copy-start.3 = (f32[256]{0:T(256)S(1)}, f32[256]{0:T(256)}, u32[]{:S(2)}) copy-start(f32[256]{0:T(256)} %param.15) | copy-start | bytes 3076
  36.9 17.7 %all-to-all-start.1 = ((bf16[4,1,768,64]{2,3,1,0:T(8,128)(2,1)}), bf16[4,1,768,64]{2,3,1,0:T(8,128)(2,1)S(1)}, u32[]{:S(2)}, u32[]{:S(2)}) async-start(bf16[4,1,768,64]{2,3,1,0:T(8,128)(2,1)} %bitcast.6), calls=%async_computation.1 | async-start | bytes 786432 | tf_op jit(solution)/shard_map/all_to_all | solution.py:48
where the time goes:
time: 56.6 us; the launch traced here: 56.2 us
  blocking collectives  24.3 us (43%)
  starting transfers between devices  9.81 us (17%)
  other arithmetic  8.65 us (15%)
  matrix products  8.39 us (15%)
  local copies, waits for them, and re-layouts  3.53 us (6%)
  between operations  1.39 us (2%)
    unnamed x1, blocking collectives  12.2 us
    psum x1, blocking collectives, read_early(): return lax.psum(partial_value, 'sp')  12.1 us
    all_to_all x1, starting transfers between devices, cache_layout(): lax.all_to_all(arrange(keys), 'sp', split_axis=0, concat_axis=1, tiled=True)  6.35 us
    another operation x2, other arithmetic  5.16 us
    dot_general x1, matrix products, project_rows(): jnp.dot(normed, value_weight, preferred_element_type=jnp.float32)  3.9 us
    all_to_all x1, starting transfers between devices, cache_layout(): lax.all_to_all(arrange(values), 'sp', split_axis=0, concat_axis=1, tiled=...  3.46 us
    reduce_sum x1, other arithmetic, normalize(): mean_square = jnp.mean(rows32 * rows32, axis=-1, keepdims=True)  2.72 us
    unnamed x20, local copies, waits for them, and re-layouts  2.51 us
  transfers between devices with their start and end apart: 2, of which 0 were waited for; matrix products, arithmetic and copies ran while one was open for 25% of the time, Pallas kernels for 0%

commit v1 on v0

--- a/solution.py
+++ b/solution.py
@@ -69,7 +69,7 @@
     sticks = jnp.exp(jax.nn.log_sigmoid(scores) + within + beyond[:, None]).astype(jnp.bfloat16)
     values3 = values.reshape(values.shape[0], head_count, depth)
     partial_value = jnp.einsum("hs,shd->hd", sticks, values3, preferred_element_type=jnp.float32)
-    return lax.psum(partial_value, "sp")
+    return jnp.sum(lax.all_gather(partial_value, "sp"), axis=0)
 
 
 def finish_read(mixed, output_gain, head_count):

time: 56.6 us -> 64.5 us (1.14)
  waiting for transfers between devices: 0.01 us -> 8.16 us
    psum x1 -> x0, blocking collectives: 12.1 us -> none  [read_early(): return lax.psum(partial_value, 'sp')]
    all_gather x0 -> x1, blocking collectives: none -> 11.9 us  [read_early(): return jnp.sum(lax.all_gather(partial_value, 'sp'), axis=0)]
    all_to_all x1, waiting for transfers between devices: 0.01 us -> 8.16 us  [cache_layout(): lax.all_to_all(arrange(values), 'sp', split_axis=0, concat_axis=1, tiled=...]
  transfers between devices with their start and end apart: 2 -> 2, of which waited for: 0 -> 1; matrix products, arithmetic and copies ran while one was open for 25% -> 21% of each run, Pallas kernels for 0% -> 0%
where the time goes in v1:
time: 64.5 us; the launch traced here: 64.1 us
  blocking collectives  24.1 us (37%)
  starting transfers between devices  9.82 us (15%)
  other arithmetic  9.17 us (14%)
  matrix products  8.41 us (13%)
  waiting for transfers between devices  8.16 us (13%)
  local copies, waits for them, and re-layouts  2.93 us (5%)
  between operations  1.4 us (2%)
    unnamed x1, blocking collectives  12.2 us
    all_gather x1, blocking collectives, read_early(): return jnp.sum(lax.all_gather(partial_value, 'sp'), axis=0)  11.9 us
    all_to_all x1, waiting for transfers between devices, cache_layout(): lax.all_to_all(arrange(values), 'sp', split_axis=0, concat_axis=1, tiled=...  8.16 us
    all_to_all x1, starting transfers between devices, cache_layout(): lax.all_to_all(arrange(keys), 'sp', split_axis=0, concat_axis=1, tiled=True)  6.35 us
    another operation x2, other arithmetic  5.16 us
    dot_general x1, matrix products, project_rows(): jnp.dot(normed, value_weight, preferred_element_type=jnp.float32)  3.95 us
    all_to_all x1, starting transfers between devices, cache_layout(): lax.all_to_all(arrange(values), 'sp', split_axis=0, concat_axis=1, tiled=...  3.47 us
    reduce_sum x1, other arithmetic, normalize(): mean_square = jnp.mean(rows32 * rows32, axis=-1, keepdims=True)  2.72 us
  transfers between devices with their start and end apart: 2, of which 1 were waited for; matrix products, arithmetic and copies ran while one was open for 21% of the time, Pallas kernels for 0%

profile of v1, /device:TPU:0, one launch (start us, length us, event | category | flops | bytes accessed | tf_op | source)
XLA Modules:
  0.0 64.1 jit_solution(161544141357022260)
XLA Ops:
  0.6 0.0 copy-start
  0.6 0.0 copy-start.1
  0.7 2.7 %fusion = f32[768]{0:T(1024)S(1)} fusion(bf16[768,2048]{1,0:T(8,128)(2,1)} %param.9), kind=kLoop, calls=%fused_computation.4 | loop fusion | flops 4717824 | bytes 3148800 | tf_op jit(solution)/shard_map/reduce_sum | solution.py:25
  3.4 0.4 copy-done.1
  3.8 0.0 copy-start.5
  3.8 2.1 %convolution_convert_fusion.1 = bf16[768,256]{0,1:T(8,128)(2,1)} fusion(bf16[2048,256]{1,0:T(8,128)(2,1)S(1)} %copy-done, bf16[768,2048]{1,0:T(8,128)(2,1)S(1)} %copy-done.1, f32[2048]{0:T(1024)S(1)} %copy-done.6, f32[768]{0:T(1024)S(1)} %add_rsqrt_fusion), kind=kOutput, calls=%fused_computation.8 | convolution fusion | flops 811794432 | bytes 4598784 | tf_op jit(solution)/shard_map/dot_general | solution.py:31
  5.9 6.3 %all-to-all-start = ((bf16[4,1,768,64]{2,3,1,0:T(8,128)(2,1)}), bf16[4,1,768,64]{2,3,1,0:T(8,128)(2,1)S(1)}, u32[]{:S(2)}, u32[]{:S(2)}) async-start(bf16[4,1,768,64]{2,3,1,0:T(8,128)(2,1)} %bitcast.2), calls=%async_computation | async-start | bytes 786432 | tf_op jit(solution)/shard_map/all_to_all | solution.py:47
  12.3 0.1 reshape.101
  12.4 1.2 %fusion.16 = f32[4,1,768]{2,1,0:T(1,128)S(1)} fusion(bf16[768,4,64]{0,2,1:T(8,128)(2,1)} %bitcast.8, bf16[4,64,1]{1,2,0:T(2,128)(2,1)S(1)} %reshape.101), kind=kOutput, calls=%fused_computation.32 | convolution fusion | flops 393216 | bytes 406016 | tf_op jit(solution)/shard_map/hd,shd->hs/dot_general | solution.py:63
  13.5 0.2 fusion.15
  13.7 5.0 %reduce-window.6 = f32[4,6,128]{2,1,0:T(8,128)S(1)} reduce-window(f32[4,6,128]{2,1,0:T(8,128)S(1)} %reshape.83, f32[]{:T(128)} %constant.61.clone.1), window={size=1x1x128 pad=0_0x0_0x0_127}, to_apply=%region_1.0 | reduce-window | flops 390144 | bytes 24580 | tf_op jit(solution)/shard_map/reduce-window
  18.7 0.1 slice_reduce_fusion
  18.8 0.2 reduce-window.9
  19.0 0.1 slice.7
  19.1 0.6 dynamic-slice
  20.3 0.1 negate_dynamic-update-slice_fusion
  20.4 12.2 %all-reduce = f32[16]{0:T(128)S(1)} all-reduce(f32[16]{0:T(128)S(1)} %negate_dynamic-update-slice_fusion), channel_id=2, replica_groups=mesh['grp'=2,'sp'=4,'tp'=4] {'sp'}, use_global_device_ids=true, to_apply=%add | all-reduce | flops 16 | bytes 128
  32.6 0.1 reshape.86
  32.7 0.1 while.16
  32.8 3.9 %convolution_convert_fusion = bf16[768,256]{0,1:T(8,128)(2,1)} fusion(bf16[2048,256]{1,0:T(8,128)(2,1)S(1)} %copy-done.5, bf16[768,2048]{1,0:T(8,128)(2,1)} %param.9, f32[2048]{0:T(1024)S(1)} %copy-done.6, f32[768]{0:T(1024)S(1)} %add_rsqrt_fusion), kind=kOutput, calls=%fused_computation.7 | convolution fusion | flops 811794432 | bytes 4598784 | tf_op jit(solution)/shard_map/dot_general | solution.py:32
  36.8 0.1 add_bitcast_fusion
  36.9 0.1 fusion.13
  37.0 1.2 %fusion.11 = f32[4,1,64]{2,1,0:T(1,128)S(1)} fusion(bf16[768,4,64]{0,2,1:T(8,128)(2,1)} %bitcast.12, bf16[4,768,1]{1,0,2:T(4,128)(2,1)S(1)} %fusion.13), kind=kOutput, calls=%fused_computation.21 | convolution fusion | flops 393216 | bytes 400384 | tf_op jit(solution)/shard_map/hs,shd->hd/dot_general | solution.py:71
  38.2 11.9 %all-gather.2 = f32[4,4,64]{2,1,0:T(4,128)S(1)} all-gather(f32[1,4,64]{2,1,0:T(4,128)S(1)} %bitcast.55), channel_id=3, replica_groups=mesh['grp'=2,'sp'=4,'tp'=4] {'sp'}, dimensions={0}, use_global_device_ids=true | all-gather | bytes 5120 | tf_op jit(solution)/shard_map/all_gather | solution.py:72
  50.1 0.1 multiply_reduce_fusion
  50.3 3.5 %all-to-all-start.1 = ((bf16[4,1,768,64]{2,3,1,0:T(8,128)(2,1)}), bf16[4,1,768,64]{2,3,1,0:T(8,128)(2,1)S(1)}, u32[]{:S(2)}, u32[]{:S(2)}) async-start(bf16[4,1,768,64]{2,3,1,0:T(8,128)(2,1)} %bitcast.6), calls=%async_computation.1 | async-start | bytes 786432 | tf_op jit(solution)/shard_map/all_to_all | solution.py:48
  53.7 0.1 broadcast_multiply_fusion
  53.8 0.1 mul.63
  53.9 0.5 multiply_convert_fusion
  54.4 8.2 %all-to-all-done.1 = bf16[4,1,768,64]{2,3,1,0:T(8,128)(2,1)S(1)} async-done(((bf16[4,1,768,64]{2,3,1,0:T(8,128)(2,1)}), bf16[4,1,768,64]{2,3,1,0:T(8,128)(2,1)S(1)}, u32[]{:S(2)}, u32[]{:S(2)}) %all-to-all-start.1) | async-done | bytes 393248 | tf_op jit(solution)/shard_map/all_to_all | solution.py:48
  62.6 0.7 %copy.46 = bf16[1,1,4,768,64]{3,4,2,1,0:T(8,128)(2,1)} copy(bf16[1,1,4,768,64]{3,4,2,1,0:T(8,128)(2,1)S(1)} %bitcast.53) | data formatting | bytes 786432
  63.3 0.7 %copy.47 = bf16[1,1,4,768,64]{3,4,2,1,0:T(8,128)(2,1)} copy(bf16[1,1,4,768,64]{3,4,2,1,0:T(8,128)(2,1)S(1)} %bitcast.54) | data formatting | bytes 786432
  (23 shorter events, 0.1 us)
Async XLA Ops:
  0.6 2.8 %copy-start = (bf16[2048,256]{1,0:T(8,128)(2,1)S(1)}, bf16[2048,256]{1,0:T(8,128)(2,1)}, u32[]{:S(2)}) copy-start(bf16[2048,256]{1,0:T(8,128)(2,1)} %param.11) | copy-start | bytes 3145732
  0.6 3.2 %copy-start.1 = (bf16[768,2048]{1,0:T(8,128)(2,1)S(1)}, bf16[768,2048]{1,0:T(8,128)(2,1)}, u32[]{:S(2)}) copy-start(bf16[768,2048]{1,0:T(8,128)(2,1)} %param.9) | copy-start | bytes 9437188
  0.7 3.1 %copy-start.6 = (f32[2048]{0:T(1024)S(1)}, f32[2048]{0:T(1024)}, u32[]{:S(2)}) copy-start(f32[2048]{0:T(1024)} %param.10) | copy-start | bytes 24580
  3.8 8.5 %copy-start.4 = (bf16[256]{0:T(256)(128)(2,1)S(1)}, bf16[256]{0:T(256)(128)(2,1)}, u32[]{:S(2)}) copy-start(bf16[256]{0:T(256)(128)(2,1)} %param.13) | copy-start | bytes 1540
  3.8 9.7 %copy-start.2 = (f32[4]{0:T(128)S(1)}, f32[4]{0:T(128)}, u32[]{:S(2)}) copy-start(f32[4]{0:T(128)} %param.14) | copy-start | bytes 52
  3.8 15.3 %copy-start.7 = (u32[32]{0:T(128)S(1)}, u32[32]{0:T(128)}, u32[]{:S(2)}) copy-start(u32[32]{0:T(128)} %constant.71) | copy-start | bytes 388
  3.8 29.0 %copy-start.5 = (bf16[2048,256]{1,0:T(8,128)(2,1)S(1)}, bf16[2048,256]{1,0:T(8,128)(2,1)}, u32[]{:S(2)}) copy-start(bf16[2048,256]{1,0:T(8,128)(2,1)} %param.12) | copy-start | bytes 3145732
  5.9 44.3 %all-to-all-start = ((bf16[4,1,768,64]{2,3,1,0:T(8,128)(2,1)}), bf16[4,1,768,64]{2,3,1,0:T(8,128)(2,1)S(1)}, u32[]{:S(2)}, u32[]{:S(2)}) async-start(bf16[4,1,768,64]{2,3,1,0:T(8,128)(2,1)} %bitcast.2), calls=%async_computation | async-start | bytes 786432 | tf_op jit(solution)/shard_map/all_to_all | solution.py:47
  32.8 21.1 %copy-start.3 = (f32[256]{0:T(256)S(1)}, f32[256]{0:T(256)}, u32[]{:S(2)}) copy-start(f32[256]{0:T(256)} %param.15) | copy-start | bytes 3076
  50.3 12.3 %all-to-all-start.1 = ((bf16[4,1,768,64]{2,3,1,0:T(8,128)(2,1)}), bf16[4,1,768,64]{2,3,1,0:T(8,128)(2,1)S(1)}, u32[]{:S(2)}, u32[]{:S(2)}) async-start(bf16[4,1,768,64]{2,3,1,0:T(8,128)(2,1)} %bitcast.6), calls=%async_computation.1 | async-start | bytes 786432 | tf_op jit(solution)/shard_map/all_to_all | solution.py:48
